TPU v7x, 32 devices: a whole 2x2x4 slice. The times are simulated.
32 devices in a mesh: sp: 4 (over y, x), tp: 8 (over z, core).
Axes of the slice: x: 2, y: 2, z: 4, core: 2. Of those that a mesh axis runs over, the one named last changes fastest.
Arguments:
- queries: bfloat16 [2048, 2048], P('sp', 'tp'), may hold values from -8 to 8
- keys: bfloat16 [2048, 1024], P('sp', 'tp'), may hold values from -8 to 8
- values: bfloat16 [2048, 1024], P('sp', 'tp'), may hold values from -6 to 6
- doc_ids: int32 [2048], P('sp'), may hold values from 0 to 1, never falling along the last dimension, each value on 1 to 1536 neighbouring positions
- sink_logits: float32 [32], P('tp'), may hold values from 3 to 6
- out_weight: bfloat16 [2048, 2048], P('tp'), may hold values from -0.75 to 0.75
- residual: bfloat16 [2048, 2048], P(('sp', 'tp')), may hold values from -6 to 6
- norm_gain: float32 [2048], replicated, may hold values from 0.1 to 1.9
- routes: int32 [2048, 2], P(('sp', 'tp')), may hold values from 0 to 3, all different within a row; in each aligned block of 64 rows (0 to 63, 64 to 127, ...) at most 36 rows name the same one
- route_weights: float32 [2048, 2], P(('sp', 'tp')), may hold values from 0.2 to 1
- gate_weight: bfloat16 [4, 2048, 7168], P('sp', None, 'tp'), may hold values from -0.125 to 0.125
- up_weight: bfloat16 [4, 2048, 7168], P('sp', None, 'tp'), may hold values from -0.125 to 0.125
- down_weight: bfloat16 [4, 7168, 2048], P('sp', 'tp'), may hold values from -0.0625 to 0.0625
Outputs:
- layer_output: bfloat16 [2048, 2048], P(('sp', 'tp'))
Inputs may be any that keep to these rules, and one draw needn't show every extreme that they name: `doc_ids`: never falling along the sequence; each document spans 1 to 1536 positions, one exactly that many. `routes`: each row names 2 different experts. In the rows of one device (aligned blocks of 64 rows) no expert is named by more than 36 rows, a bound that some block reaches.
All inputs are finite; a program needn't handle non-finite values.
Results may differ from a plain program's by a relative error of at most 0.015.
Values may be sent and summed in bfloat16 or wider, within the bound.
A program may use at most 128 MiB of HBM per device.

v0:
```python
import math
import jax
import jax.numpy as jnp
from jax import lax
from jax.sharding import PartitionSpec as P

HEAD_DIM = 64
WINDOW = 128
layer_epsilon = 1e-05
masked_score = -1e30


def passed_along(value, axis, steps):
    count = lax.axis_size(axis)
    first, last = (max(0, -steps), min(count, count - steps))
    return lax.ppermute(value, axis, [(source, source + steps) for source in range(first, last)])


def local(
    queries,
    keys,
    values,
    doc_ids,
    sink_logits,
    out_weight,
    residual,
    norm_gain,
    routes,
    route_weights,
    gate_weight,
    up_weight,
    down_weight,
):
    span_rows = queries.shape[0]
    kv_width = keys.shape[1]
    kv_groups = kv_width // HEAD_DIM
    heads_here = queries.shape[1] // HEAD_DIM
    group_ratio = heads_here // kv_groups
    reach_back = WINDOW - 1
    score_scale = 1.0 / math.sqrt(HEAD_DIM)
    doc_float = (doc_ids + 1).astype(jnp.float32)
    key_value = jnp.concatenate([keys, values], axis=1).astype(jnp.float32)
    tail_pairs, tail_docs = (
        passed_along(key_value[span_rows - reach_back :].astype(jnp.bfloat16), "sp", 1).astype(
            jnp.float32
        ),
        passed_along(doc_float[span_rows - reach_back :].astype(jnp.bfloat16), "sp", 1).astype(
            jnp.float32
        ),
    )
    all_keys = jnp.concatenate([tail_pairs[:, :kv_width].astype(jnp.bfloat16), keys], axis=0)
    all_values = jnp.concatenate([tail_pairs[:, kv_width:].astype(jnp.bfloat16), values], axis=0)
    all_docs = jnp.concatenate([tail_docs, doc_float], axis=0)
    block_rows = min(512, span_rows)
    sink_table = sink_logits.reshape(kv_groups, group_ratio, 1)
    offsets = (
        jnp.arange(block_rows)[:, None] + reach_back - jnp.arange(block_rows + reach_back)[None, :]
    )
    window_mask = (offsets >= 0) & (offsets <= reach_back)
    pieces = []
    for block_index in range(span_rows // block_rows):
        first_row = block_index * block_rows
        query_rows = queries[first_row : first_row + block_rows].reshape(
            block_rows, kv_groups, group_ratio, HEAD_DIM
        )
        key_rows = all_keys[first_row : first_row + block_rows + reach_back].reshape(
            block_rows + reach_back, kv_groups, HEAD_DIM
        )
        value_rows = all_values[first_row : first_row + block_rows + reach_back].reshape(
            block_rows + reach_back, kv_groups, HEAD_DIM
        )
        scores = (
            jnp.einsum("bgrd,sgd->grbs", query_rows, key_rows, preferred_element_type=jnp.float32)
            * score_scale
        )
        same_doc = (
            doc_float[first_row : first_row + block_rows][:, None]
            == all_docs[first_row : first_row + block_rows + reach_back][None, :]
        )
        scores = jnp.where(window_mask & same_doc, scores, masked_score)
        row_max = jnp.maximum(scores.max(-1), sink_table)
        exp_scores = jnp.exp(scores - row_max[..., None])
        denominator = exp_scores.sum(-1) + jnp.exp(sink_table - row_max)
        weighted = jnp.einsum(
            "grbs,sgd->bgrd",
            exp_scores.astype(jnp.bfloat16),
            value_rows,
            preferred_element_type=jnp.float32,
        )
        weighted = weighted / jnp.transpose(denominator, (2, 0, 1))[..., None]
        pieces.append(weighted.astype(jnp.bfloat16).reshape(block_rows, heads_here * HEAD_DIM))
    attended = jnp.concatenate(pieces, axis=0)
    rows_here = attended
    projected = lax.psum_scatter(
        jnp.dot(rows_here, out_weight, preferred_element_type=jnp.float32).astype(jnp.bfloat16),
        "tp",
        scatter_dimension=0,
        tiled=True,
    ).astype(jnp.float32)
    stream = residual.astype(jnp.float32) + projected
    mean_value = stream.mean(-1, keepdims=True)
    centred = stream - mean_value
    variance = (centred * centred).mean(-1, keepdims=True)
    normed = (centred * lax.rsqrt(variance + layer_epsilon) * norm_gain).astype(jnp.bfloat16)
    token_count = residual.shape[0]
    width = residual.shape[1]
    route_count = routes.shape[1]
    expert_count = lax.axis_size("sp") * gate_weight.shape[0]
    capacity = 9 * route_count * token_count // (8 * expert_count)
    flat_routes = routes.reshape(-1)
    one_hot = (flat_routes[:, None] == jnp.arange(expert_count)[None, :]).astype(jnp.int32)
    slot_ids = jnp.sum((jnp.cumsum(one_hot, axis=0) - 1) * one_hot, axis=1)
    destination = flat_routes * capacity + slot_ids
    slot_range = jnp.arange(expert_count * capacity)
    selector = jnp.any(
        slot_range[:, None, None] == destination.reshape(token_count, route_count)[None], axis=2
    )
    dispatch = jnp.dot(
        selector.astype(jnp.bfloat16), normed, preferred_element_type=jnp.float32
    ).astype(jnp.bfloat16)
    inbound = lax.all_to_all(
        dispatch.reshape(expert_count, capacity, width),
        "sp",
        split_axis=0,
        concat_axis=0,
        tiled=True,
    )
    arrived = inbound.reshape(-1, width)
    row_piece = lax.all_gather(arrived, "tp", axis=0, tiled=True)
    gate = jnp.dot(row_piece, gate_weight[0], preferred_element_type=jnp.float32)
    upward = jnp.dot(row_piece, up_weight[0], preferred_element_type=jnp.float32)
    hidden = (jax.nn.silu(gate) * upward).astype(jnp.bfloat16)
    rows_here = hidden
    partial_value = jnp.dot(rows_here, down_weight[0], preferred_element_type=jnp.float32).astype(
        jnp.bfloat16
    )
    returned = lax.psum_scatter(
        lax.optimization_barrier(partial_value).astype(jnp.float32).astype(jnp.bfloat16),
        "tp",
        scatter_dimension=0,
        tiled=True,
    )
    back_rows = lax.all_to_all(
        returned.reshape(inbound.shape), "sp", split_axis=0, concat_axis=0, tiled=True
    ).reshape(-1, width)
    picked = back_rows[destination].astype(jnp.float32).reshape(token_count, route_count, width)
    combined = jnp.sum(picked * route_weights[..., None], axis=1)
    return (stream + combined).astype(jnp.bfloat16)


def solution(mesh):
    placed = (
        P("sp", "tp"),
        P("sp", "tp"),
        P("sp", "tp"),
        P("sp"),
        P("tp"),
        P("tp", None),
        P(("sp", "tp"), None),
        P(),
        P(("sp", "tp"), None),
        P(("sp", "tp"), None),
        P("sp", None, "tp"),
        P("sp", None, "tp"),
        P("sp", "tp", None),
    )
    return jax.shard_map(
        local, mesh=mesh, in_specs=placed, out_specs=P(("sp", "tp"), None), check_vma=False
    )
```

profile of v0, /device:TPU:0, one launch (start us, length us, event | category | flops | bytes accessed | tf_op | source)
XLA Modules:
  0.0 232.7 jit_solution(13959658188333084272)
XLA Ops:
  6.5 0.8 fusion.35
  7.4 4.9 %collective-permute-start.1 = (bf16[127]{0:T(256)(128)(2,1)S(1)}, bf16[127]{0:T(256)(128)(2,1)S(1)}, u32[]{:S(2)}, u32[]{:S(2)}) collective-permute-start(bf16[127]{0:T(256)(128)(2,1)S(1)} %slice.18), channel_id=1, source_target_pairs={{0,8},{8,16},{16,24},{1,9},{9,17},{17,25},{2,10},{10,18},{18,26},{... | collective-permute-start | bytes 770 | tf_op jit(solution)/shard_map/ppermute | solution.py:16
  12.3 0.8 pad_maximum_fusion.2
  13.1 3.4 %collective-permute-start = (bf16[127,256]{1,0:T(8,128)(2,1)S(1)}, bf16[127,256]{1,0:T(8,128)(2,1)S(1)}, u32[]{:S(2)}, u32[]{:S(2)}) collective-permute-start(bf16[127,256]{1,0:T(8,128)(2,1)S(1)} %pad_maximum_fusion.2), channel_id=1, source_target_pairs={{0,8},{8,16},{16,24},{1,9},{9,17},{17,25},{2,10},{10,18},{18,26},{... | collective-permute-start | bytes 195080 | tf_op jit(solution)/shard_map/ppermute | solution.py:16
  16.5 1.1 copy.30
  17.6 0.7 max.16
  18.4 0.5 fusion.16
  18.9 1.0 pad_maximum_fusion
  20.1 1.1 fusion.2
  21.3 2.2 copy-done.1
  23.5 1.1 fusion
  24.9 4.0 %fusion.23 = bf16[512,2,2,64]{0,3,2,1:T(8,128)(2,1)S(1)} fusion(bf16[639,2,64,1]{0,2,3,1:T(8,128)(2,1)S(1)} %bitcast.63, f32[2,639,512,2]{2,1,3,0:T(8,128)} %copy-done.1, f32[2,2,512]{2,1,0:T(2,128)S(1)} %broadcast_maximum_fusion, pred[512,639]{0,1:T(8,128)(4,1)S(1)} %fusion.16, f32[512,2,2]{0,2,1:T(2,128)S(1)} %add_bitcast_fusion), kind=kOutput, calls=%fused_computation.25 | convolution fusion | flops 173006848 | bytes 6003968 | tf_op jit(solution)/shard_map/grbs,sgd->bgrd/dot_general | solution.py:84
  28.9 2.1 convolution_convert_fusion.1
  32.1 36.7 %reduce-scatter.3.cloned.1.call-done = bf16[64,2048]{1,0:T(8,128)(2,1)} async-done(((bf16[512,2048]{1,0:T(8,128)(2,1)}), bf16[64,2048]{1,0:T(8,128)(2,1)}) %reduce-scatter.3.cloned.1.call-update) | async-done | bytes 262160 | tf_op jit(solution)/shard_map/reduce_scatter | solution.py:94
  68.8 1.1 fusion.26
  70.0 1.2 multiply_reduce_fusion.1
  71.2 1.3 convolution_convert_fusion.2
  72.7 11.1 %all_to_all.10 = bf16[4,36,2048]{2,1,0:T(8,128)(2,1)S(1)} all-to-all(bf16[4,36,2048]{2,1,0:T(8,128)(2,1)S(1)} %reshape.95), channel_id=1, replica_groups=mesh['sp'=4,'tp'=8] {'sp'}, dimensions={0} | all-to-all | bytes 1179648 | tf_op jit(solution)/shard_map/all_to_all | solution.py:121
  83.8 1.0 reshape.96
  84.7 0.2 reduce-scatter.5.cloned.1.call-start
  85.0 49.7 %all-gather.2.cloned.1.call-done = bf16[1152,2048]{1,0:T(8,128)(2,1)} async-done(((bf16[144,2048]{1,0:T(8,128)(2,1)}), bf16[1152,2048]{1,0:T(8,128)(2,1)}) %all-gather.2.cloned.1.call-update) | async-done | bytes 4718608 | tf_op jit(solution)/shard_map/all_gather | solution.py:129
  134.7 8.1 %fusion.5 = f32[1152,896]{1,0:T(8,128)S(1)} fusion(bf16[1152,2048]{1,0:T(8,128)(2,1)} %all-gather.2.cloned.1.call-done, bf16[1,2048,896]{2,1,0:T(8,128)(2,1)} %param.23), kind=kOutput, calls=%fused_computation.10 | convolution fusion | flops 4227858432 | bytes 12517376 | tf_op jit(solution)/shard_map/dot_general | solution.py:130
  142.8 5.3 %fusion.7 = bf16[1152,896]{1,0:T(8,128)(2,1)S(1)} fusion(bf16[1152,2048]{1,0:T(8,128)(2,1)S(1)} %copy-done.7, bf16[1,2048,896]{2,1,0:T(8,128)(2,1)S(1)} %copy-done.8, f32[1152,896]{1,0:T(8,128)S(1)} %fusion.5), kind=kOutput, calls=%fused_computation.12 | convolution fusion | flops 4234051584 | bytes 14581760 | tf_op jit(solution)/shard_map/dot_general | solution.py:131
  148.2 6.7 %convolution_convert_fusion = bf16[1152,2048]{1,0:T(8,128)(2,1)} fusion(bf16[1152,896]{1,0:T(8,128)(2,1)S(1)} %fusion.7, bf16[1,896,2048]{2,1,0:T(8,128)(2,1)S(1)} %copy-done.9), kind=kOutput, calls=%fused_computation.1 | convolution fusion | flops 4230217728 | bytes 10452992 | tf_op jit(solution)/shard_map/dot_general | solution.py:134
  154.9 53.8 %reduce-scatter.5.cloned.1.call-done = bf16[144,2048]{1,0:T(8,128)(2,1)} async-done(((bf16[1152,2048]{1,0:T(8,128)(2,1)}), bf16[144,2048]{1,0:T(8,128)(2,1)}) %reduce-scatter.5.cloned.1.call-update) | async-done | bytes 589840 | tf_op jit(solution)/shard_map/reduce_scatter | solution.py:137
  208.7 2.0 reshape.97
  210.7 3.6 %all-to-all-start.1 = ((bf16[4,36,2048]{2,1,0:T(8,128)(2,1)}), bf16[4,36,2048]{2,1,0:T(8,128)(2,1)S(1)}, u32[]{:S(2)}, u32[]{:S(2)}) async-start(bf16[4,36,2048]{2,1,0:T(8,128)(2,1)} %reshape.97), calls=%async_computation.3 | async-start | bytes 1310720 | tf_op jit(solution)/shard_map/all_to_all | solution.py:143
  214.6 7.4 %all-to-all-done.1 = bf16[4,36,2048]{2,1,0:T(8,128)(2,1)S(1)} async-done(((bf16[4,36,2048]{2,1,0:T(8,128)(2,1)}), bf16[4,36,2048]{2,1,0:T(8,128)(2,1)S(1)}, u32[]{:S(2)}, u32[]{:S(2)}) %all-to-all-start.1) | async-done | bytes 589856 | tf_op jit(solution)/shard_map/all_to_all | solution.py:143
  222.2 0.9 gather_fusion
  223.1 0.7 reshape.99
  223.8 1.5 multiply_reduce_fusion
  225.3 0.8 add_convert_fusion
  (52 shorter events, 2.3 us)
Async XLA Ops:
  6.5 22.4 %copy-start = (bf16[256,2048]{1,0:T(8,128)(2,1)S(1)}, bf16[256,2048]{1,0:T(8,128)(2,1)}, u32[]{:S(2)}) copy-start(bf16[256,2048]{1,0:T(8,128)(2,1)} %param.18) | copy-start | bytes 3145732
  6.5 62.3 %reduce-scatter.3.cloned.1.call-start = ((), (), s32[]{:S(2)}) async-start(), calls=%async_computation.4 | async-start | bytes 2359296 | tf_op jit(solution)/shard_map/reduce_scatter | solution.py:94
  7.4 10.9 %collective-permute-start.1 = (bf16[127]{0:T(256)(128)(2,1)S(1)}, bf16[127]{0:T(256)(128)(2,1)S(1)}, u32[]{:S(2)}, u32[]{:S(2)}) collective-permute-start(bf16[127]{0:T(256)(128)(2,1)S(1)} %slice.18), channel_id=1, source_target_pairs={{0,8},{8,16},{16,24},{1,9},{9,17},{17,25},{2,10},{10,18},{18,26},{... | collective-permute-start | bytes 770 | tf_op jit(solution)/shard_map/ppermute | solution.py:16
  13.1 5.8 %collective-permute-start = (bf16[127,256]{1,0:T(8,128)(2,1)S(1)}, bf16[127,256]{1,0:T(8,128)(2,1)S(1)}, u32[]{:S(2)}, u32[]{:S(2)}) collective-permute-start(bf16[127,256]{1,0:T(8,128)(2,1)S(1)} %pad_maximum_fusion.2), channel_id=1, source_target_pairs={{0,8},{8,16},{16,24},{1,9},{9,17},{17,25},{2,10},{10,18},{18,26},{... | collective-permute-start | bytes 195080 | tf_op jit(solution)/shard_map/ppermute | solution.py:16
  21.2 2.3 copy-start.1
  28.9 2.2 copy-start.5
  28.9 40.0 %copy-start.2 = (bf16[64,2048]{1,0:T(8,128)(2,1)S(1)}, bf16[64,2048]{1,0:T(8,128)(2,1)}, u32[]{:S(2)}) copy-start(bf16[64,2048]{1,0:T(8,128)(2,1)} %param.19) | copy-start | bytes 786436
  28.9 42.3 %copy-start.4 = (f32[2048]{0:T(1024)S(1)}, f32[2048]{0:T(1024)}, u32[]{:S(2)}) copy-start(f32[2048]{0:T(1024)} %param.20) | copy-start | bytes 24580
  31.0 103.7 %all-gather.2.cloned.1.call-start = ((), (), s32[]{:S(2)}) async-start(), calls=%async_computation.5 | async-start | bytes 5308416 | tf_op jit(solution)/shard_map/all_gather | solution.py:129
  84.7 124.0 %reduce-scatter.5.cloned.1.call-start = ((), (), s32[]{:S(2)}) async-start(), calls=%async_computation.6 | async-start | bytes 5308416 | tf_op jit(solution)/shard_map/reduce_scatter | solution.py:137
  134.7 8.1 %copy-start.7 = (bf16[1152,2048]{1,0:T(8,128)(2,1)S(1)}, bf16[1152,2048]{1,0:T(8,128)(2,1)}, u32[]{:S(2)}) copy-start(bf16[1152,2048]{1,0:T(8,128)(2,1)} %all-gather.2.cloned.1.call-done) | copy-start | bytes 14155780
  134.7 8.1 %copy-start.8 = (bf16[1,2048,896]{2,1,0:T(8,128)(2,1)S(1)}, bf16[1,2048,896]{2,1,0:T(8,128)(2,1)}, u32[]{:S(2)}) copy-start(bf16[1,2048,896]{2,1,0:T(8,128)(2,1)} %param.24) | copy-start | bytes 11010052
  142.8 5.3 %copy-start.9 = (bf16[1,896,2048]{2,1,0:T(8,128)(2,1)S(1)}, bf16[1,896,2048]{2,1,0:T(8,128)(2,1)}, u32[]{:S(2)}) copy-start(bf16[1,896,2048]{2,1,0:T(8,128)(2,1)} %param.25) | copy-start | bytes 11010052
  154.9 59.6 %copy-start.6 = (f32[64,2]{0,1:T(2,128)S(1)}, f32[64,2]{0,1:T(2,128)}, u32[]{:S(2)}) copy-start(f32[64,2]{0,1:T(2,128)} %param.22) | copy-start | bytes 1540
  210.7 11.3 %all-to-all-start.1 = ((bf16[4,36,2048]{2,1,0:T(8,128)(2,1)}), bf16[4,36,2048]{2,1,0:T(8,128)(2,1)S(1)}, u32[]{:S(2)}, u32[]{:S(2)}) async-start(bf16[4,36,2048]{2,1,0:T(8,128)(2,1)} %reshape.97), calls=%async_computation.3 | async-start | bytes 1310720 | tf_op jit(solution)/shard_map/all_to_all | solution.py:143
  222.2 3.2 %copy-start.3 = (bf16[64,2048]{1,0:T(8,128)(2,1)S(1)}, bf16[64,2048]{1,0:T(8,128)(2,1)}, u32[]{:S(2)}) copy-start(bf16[64,2048]{1,0:T(8,128)(2,1)} %reduce-scatter.3.cloned.1.call-done) | copy-start | bytes 786436
Sparse Core Ops, SparseCore 0:
  31.1 37.6 reduce-scatter.2
  84.9 49.7 all-gather.1
  155.0 53.6 reduce-scatter.4
where the time goes:
time: 233 us
  waiting for transfers between devices  148 us (64%)
  matrix products  28.7 us (12%)
  between operations  13.4 us (6%)
  starting transfers between devices  12.2 us (5%)
  blocking collectives  11.1 us (5%)
  local copies, waits for them, and re-layouts  9.98 us (4%)
  other arithmetic  9.64 us (4%)
    reduce_scatter x1, waiting for transfers between devices, local(): lax.psum_scatter(lax.optimization_barrier(partial_value).astype(jnp.float...  53.8 us
    all_gather x1, waiting for transfers between devices, local(): row_piece = lax.all_gather(arrived, 'tp', axis=0, tiled=True)  49.7 us
    reduce_scatter x1, waiting for transfers between devices, local(): lax.psum_scatter(jnp.dot(rows_here, out_weight, preferred_element_type=jn...  36.7 us
    all_to_all x1, blocking collectives, local(): lax.all_to_all(dispatch.reshape(expert_count, capacity, width), 'sp', spl...  11.1 us
    ppermute x2, starting transfers between devices, passed_along(): lax.ppermute(value, axis, [(source, source + steps) for source in range(f...  8.26 us
    dot_general x1, matrix products, local(): jnp.dot(row_piece, gate_weight[0], preferred_element_type=jnp.float32)  8.11 us
    all_to_all x1, waiting for transfers between devices, local(): lax.all_to_all(returned.reshape(inbound.shape), 'sp', split_axis=0, conca...  7.42 us
    dot_general x1, matrix products, local(): jnp.dot(rows_here, down_weight[0], preferred_element_type=jnp.float32)  6.73 us
  transfers between devices with their start and end apart: 6, of which 4 were waited for; matrix products, arithmetic and copies ran while one was open for 2% of the time, Pallas kernels for 0%

commit v1 on v0

--- a/solution.py
+++ b/solution.py
@@ -126,7 +126,10 @@
         tiled=True,
     )
     arrived = inbound.reshape(-1, width)
-    row_piece = lax.all_gather(arrived, "tp", axis=0, tiled=True)
+    size = lax.axis_size("tp")
+    blocks = jnp.stack([arrived for _ in range(size)])
+    blocks = lax.all_to_all(blocks, "tp", split_axis=0, concat_axis=0)
+    row_piece = jnp.concatenate(blocks, axis=0)
     gate = jnp.dot(row_piece, gate_weight[0], preferred_element_type=jnp.float32)
     upward = jnp.dot(row_piece, up_weight[0], preferred_element_type=jnp.float32)
     hidden = (jax.nn.silu(gate) * upward).astype(jnp.bfloat16)

time: 233 us -> 288 us (1.24)
  blocking collectives: 11.1 us -> 120 us
  waiting for transfers between devices: 148 us -> 96.6 us
  matrix products: 28.7 us -> 25.6 us
    all_to_all x0 -> x1, blocking collectives: none -> 109 us  [local(): blocks = lax.all_to_all(blocks, 'tp', split_axis=0, concat_axis=0)]
    all_gather x1 -> x0, waiting for transfers between devices: 49.7 us -> none  [local(): row_piece = lax.all_gather(arrived, 'tp', axis=0, tiled=True)]
    dot_general x1, matrix products: 8.11 us -> 5.09 us  [local(): jnp.dot(row_piece, gate_weight[0], preferred_element_type=jnp.float32)]
  transfers between devices with their start and end apart: 6 -> 5, of which waited for: 4 -> 3; matrix products, arithmetic and copies ran while one was open for 2% -> 2% of each run, Pallas kernels for 0% -> 0%
where the time goes in v1:
time: 288 us; the launch traced here: 287 us
  blocking collectives  120 us (42%)
  waiting for transfers between devices  96.6 us (34%)
  matrix products  25.6 us (9%)
  between operations  13.7 us (5%)
  starting transfers between devices  12 us (4%)
  local copies, waits for them, and re-layouts  9.74 us (3%)
  other arithmetic  9.64 us (3%)
    all_to_all x1, blocking collectives, local(): blocks = lax.all_to_all(blocks, 'tp', split_axis=0, concat_axis=0)  109 us
    reduce_scatter x1, waiting for transfers between devices, local(): lax.psum_scatter(lax.optimization_barrier(partial_value).astype(jnp.float...  52.4 us
    reduce_scatter x1, waiting for transfers between devices, local(): lax.psum_scatter(jnp.dot(rows_here, out_weight, preferred_element_type=jn...  36.7 us
    all_to_all x1, blocking collectives, local(): lax.all_to_all(dispatch.reshape(expert_count, capacity, width), 'sp', spl...  11.1 us
    ppermute x2, starting transfers between devices, passed_along(): lax.ppermute(value, axis, [(source, source + steps) for source in range(f...  8.26 us
    all_to_all x1, waiting for transfers between devices, local(): lax.all_to_all(returned.reshape(inbound.shape), 'sp', split_axis=0, conca...  7.41 us
    dot_general x1, matrix products, local(): jnp.dot(rows_here, down_weight[0], preferred_element_type=jnp.float32)  6.73 us
  transfers between devices with their start and end apart: 5, of which 3 were waited for; matrix products, arithmetic and copies ran while one was open for 2% of the time, Pallas kernels for 0%

profile of v1, /device:TPU:0, one launch (start us, length us, event | category | flops | bytes accessed | tf_op | source)
XLA Modules:
  0.0 287.4 jit_solution(17932901524983826513)
XLA Ops:
  6.5 0.8 fusion.35
  7.4 4.9 %collective-permute-start.1 = (bf16[127]{0:T(256)(128)(2,1)S(1)}, bf16[127]{0:T(256)(128)(2,1)S(1)}, u32[]{:S(2)}, u32[]{:S(2)}) collective-permute-start(bf16[127]{0:T(256)(128)(2,1)S(1)} %slice.18), channel_id=1, source_target_pairs={{0,8},{8,16},{16,24},{1,9},{9,17},{17,25},{2,10},{10,18},{18,26},{... | collective-permute-start | bytes 770 | tf_op jit(solution)/shard_map/ppermute | solution.py:16
  12.3 0.8 pad_maximum_fusion.2
  13.1 3.4 %collective-permute-start = (bf16[127,256]{1,0:T(8,128)(2,1)S(1)}, bf16[127,256]{1,0:T(8,128)(2,1)S(1)}, u32[]{:S(2)}, u32[]{:S(2)}) collective-permute-start(bf16[127,256]{1,0:T(8,128)(2,1)S(1)} %pad_maximum_fusion.2), channel_id=1, source_target_pairs={{0,8},{8,16},{16,24},{1,9},{9,17},{17,25},{2,10},{10,18},{18,26},{... | collective-permute-start | bytes 195080 | tf_op jit(solution)/shard_map/ppermute | solution.py:16
  16.5 1.1 copy.30
  17.6 0.7 max.16
  18.4 0.5 fusion.16
  18.9 1.0 pad_maximum_fusion
  20.1 1.1 fusion.2
  21.3 2.2 copy-done.1
  23.5 1.1 fusion
  24.9 4.0 %fusion.23 = bf16[512,2,2,64]{0,3,2,1:T(8,128)(2,1)S(1)} fusion(bf16[639,2,64,1]{0,2,3,1:T(8,128)(2,1)S(1)} %bitcast.66, f32[2,639,512,2]{2,1,3,0:T(8,128)} %copy-done.1, f32[2,2,512]{2,1,0:T(2,128)S(1)} %broadcast_maximum_fusion, pred[512,639]{0,1:T(8,128)(4,1)S(1)} %fusion.16, f32[512,2,2]{0,2,1:T(2,128)S(1)} %add_bitcast_fusion), kind=kOutput, calls=%fused_computation.25 | convolution fusion | flops 173006848 | bytes 6003968 | tf_op jit(solution)/shard_map/grbs,sgd->bgrd/dot_general | solution.py:84
  28.9 2.1 convolution_convert_fusion.1
  31.4 0.2 reduce_window_sum.11
  32.1 36.7 %reduce-scatter.3.cloned.1.call-done = bf16[64,2048]{1,0:T(8,128)(2,1)} async-done(((bf16[512,2048]{1,0:T(8,128)(2,1)}), bf16[64,2048]{1,0:T(8,128)(2,1)}) %reduce-scatter.3.cloned.1.call-update) | async-done | bytes 262160 | tf_op jit(solution)/shard_map/reduce_scatter | solution.py:94
  68.8 1.1 fusion.26
  70.0 1.2 multiply_reduce_fusion.1
  71.2 1.3 convolution_convert_fusion.2
  72.7 11.1 %all_to_all.15 = bf16[4,36,2048]{2,1,0:T(8,128)(2,1)S(1)} all-to-all(bf16[4,36,2048]{2,1,0:T(8,128)(2,1)S(1)} %reshape.97), channel_id=1, replica_groups=mesh['sp'=4,'tp'=8] {'sp'}, dimensions={0} | all-to-all | bytes 1179648 | tf_op jit(solution)/shard_map/all_to_all | solution.py:121
  83.9 0.6 stack.3
  84.5 109.0 %all_to_all.16 = bf16[8,144,2048]{2,1,0:T(8,128)(2,1)S(1)} all-to-all(bf16[8,144,2048]{2,1,0:T(8,128)(2,1)S(1)} %stack.3), channel_id=1, replica_groups=mesh['sp'=4,'tp'=8] {'tp'}, dimensions={0} | all-to-all | bytes 9437184 | tf_op jit(solution)/shard_map/all_to_all | solution.py:131
  193.5 5.1 %fusion.5 = f32[1152,896]{1,0:T(8,128)S(1)} fusion(bf16[1152,2048]{1,0:T(8,128)(2,1)S(1)} %bitcast.62, bf16[1,2048,896]{2,1,0:T(8,128)(2,1)S(1)} %copy-done.7), kind=kOutput, calls=%fused_computation.10 | convolution fusion | flops 4227858432 | bytes 12517376 | tf_op jit(solution)/shard_map/dot_general | solution.py:133
  198.6 5.3 %fusion.7 = bf16[1152,896]{1,0:T(8,128)(2,1)S(1)} fusion(bf16[1152,2048]{1,0:T(8,128)(2,1)S(1)} %bitcast.63, bf16[1,2048,896]{2,1,0:T(8,128)(2,1)S(1)} %copy-done.8, f32[1152,896]{1,0:T(8,128)S(1)} %fusion.5), kind=kOutput, calls=%fused_computation.12 | convolution fusion | flops 4234051584 | bytes 14581760 | tf_op jit(solution)/shard_map/dot_general | solution.py:134
  203.9 6.7 %convolution_convert_fusion = bf16[1152,2048]{1,0:T(8,128)(2,1)} fusion(bf16[1152,896]{1,0:T(8,128)(2,1)S(1)} %fusion.7, bf16[1,896,2048]{2,1,0:T(8,128)(2,1)S(1)} %copy-done.9), kind=kOutput, calls=%fused_computation.1 | convolution fusion | flops 4230217728 | bytes 10452992 | tf_op jit(solution)/shard_map/dot_general | solution.py:137
  210.7 52.4 %reduce-scatter.5.cloned.1.call-done = bf16[144,2048]{1,0:T(8,128)(2,1)} async-done(((bf16[1152,2048]{1,0:T(8,128)(2,1)}), bf16[144,2048]{1,0:T(8,128)(2,1)}) %reduce-scatter.5.cloned.1.call-update) | async-done | bytes 589840 | tf_op jit(solution)/shard_map/reduce_scatter | solution.py:140
  263.1 2.0 reshape.99
  265.1 3.6 %all-to-all-start.2 = ((bf16[4,36,2048]{2,1,0:T(8,128)(2,1)}), bf16[4,36,2048]{2,1,0:T(8,128)(2,1)S(1)}, u32[]{:S(2)}, u32[]{:S(2)}) async-start(bf16[4,36,2048]{2,1,0:T(8,128)(2,1)} %reshape.99), calls=%async_computation.4 | async-start | bytes 1310720 | tf_op jit(solution)/shard_map/all_to_all | solution.py:146
  269.0 7.4 %all-to-all-done.2 = bf16[4,36,2048]{2,1,0:T(8,128)(2,1)S(1)} async-done(((bf16[4,36,2048]{2,1,0:T(8,128)(2,1)}), bf16[4,36,2048]{2,1,0:T(8,128)(2,1)S(1)}, u32[]{:S(2)}, u32[]{:S(2)}) %all-to-all-start.2) | async-done | bytes 589856 | tf_op jit(solution)/shard_map/all_to_all | solution.py:146
  276.6 0.9 gather_fusion
  277.5 0.7 reshape.101
  278.2 1.5 multiply_reduce_fusion
  279.7 0.8 add_convert_fusion
  (51 shorter events, 2.2 us)
Async XLA Ops:
  6.5 22.4 %copy-start = (bf16[256,2048]{1,0:T(8,128)(2,1)S(1)}, bf16[256,2048]{1,0:T(8,128)(2,1)}, u32[]{:S(2)}) copy-start(bf16[256,2048]{1,0:T(8,128)(2,1)} %param.18) | copy-start | bytes 3145732
  6.5 62.3 %reduce-scatter.3.cloned.1.call-start = ((), (), s32[]{:S(2)}) async-start(), calls=%async_computation.5 | async-start | bytes 2359296 | tf_op jit(solution)/shard_map/reduce_scatter | solution.py:94
  7.4 10.9 %collective-permute-start.1 = (bf16[127]{0:T(256)(128)(2,1)S(1)}, bf16[127]{0:T(256)(128)(2,1)S(1)}, u32[]{:S(2)}, u32[]{:S(2)}) collective-permute-start(bf16[127]{0:T(256)(128)(2,1)S(1)} %slice.18), channel_id=1, source_target_pairs={{0,8},{8,16},{16,24},{1,9},{9,17},{17,25},{2,10},{10,18},{18,26},{... | collective-permute-start | bytes 770 | tf_op jit(solution)/shard_map/ppermute | solution.py:16
  13.1 5.8 %collective-permute-start = (bf16[127,256]{1,0:T(8,128)(2,1)S(1)}, bf16[127,256]{1,0:T(8,128)(2,1)S(1)}, u32[]{:S(2)}, u32[]{:S(2)}) collective-permute-start(bf16[127,256]{1,0:T(8,128)(2,1)S(1)} %pad_maximum_fusion.2), channel_id=1, source_target_pairs={{0,8},{8,16},{16,24},{1,9},{9,17},{17,25},{2,10},{10,18},{18,26},{... | collective-permute-start | bytes 195080 | tf_op jit(solution)/shard_map/ppermute | solution.py:16
  21.2 2.3 copy-start.1
  28.9 2.2 copy-start.5
  28.9 40.0 %copy-start.2 = (bf16[64,2048]{1,0:T(8,128)(2,1)S(1)}, bf16[64,2048]{1,0:T(8,128)(2,1)}, u32[]{:S(2)}) copy-start(bf16[64,2048]{1,0:T(8,128)(2,1)} %param.19) | copy-start | bytes 786436
  28.9 42.3 %copy-start.4 = (f32[2048]{0:T(1024)S(1)}, f32[2048]{0:T(1024)}, u32[]{:S(2)}) copy-start(f32[2048]{0:T(1024)} %param.20) | copy-start | bytes 24580
  31.0 232.1 %reduce-scatter.5.cloned.1.call-start = ((), (), s32[]{:S(2)}) async-start(), calls=%async_computation.6 | async-start | bytes 5308416 | tf_op jit(solution)/shard_map/reduce_scatter | solution.py:140
  84.5 109.0 %copy-start.7 = (bf16[1,2048,896]{2,1,0:T(8,128)(2,1)S(1)}, bf16[1,2048,896]{2,1,0:T(8,128)(2,1)}, u32[]{:S(2)}) copy-start(bf16[1,2048,896]{2,1,0:T(8,128)(2,1)} %param.23) | copy-start | bytes 11010052
  193.5 5.1 %copy-start.8 = (bf16[1,2048,896]{2,1,0:T(8,128)(2,1)S(1)}, bf16[1,2048,896]{2,1,0:T(8,128)(2,1)}, u32[]{:S(2)}) copy-start(bf16[1,2048,896]{2,1,0:T(8,128)(2,1)} %param.24) | copy-start | bytes 11010052
  198.6 5.3 %copy-start.9 = (bf16[1,896,2048]{2,1,0:T(8,128)(2,1)S(1)}, bf16[1,896,2048]{2,1,0:T(8,128)(2,1)}, u32[]{:S(2)}) copy-start(bf16[1,896,2048]{2,1,0:T(8,128)(2,1)} %param.25) | copy-start | bytes 11010052
  210.7 58.3 %copy-start.6 = (f32[64,2]{0,1:T(2,128)S(1)}, f32[64,2]{0,1:T(2,128)}, u32[]{:S(2)}) copy-start(f32[64,2]{0,1:T(2,128)} %param.22) | copy-start | bytes 1540
  265.1 11.3 %all-to-all-start.2 = ((bf16[4,36,2048]{2,1,0:T(8,128)(2,1)}), bf16[4,36,2048]{2,1,0:T(8,128)(2,1)S(1)}, u32[]{:S(2)}, u32[]{:S(2)}) async-start(bf16[4,36,2048]{2,1,0:T(8,128)(2,1)} %reshape.99), calls=%async_computation.4 | async-start | bytes 1310720 | tf_op jit(solution)/shard_map/all_to_all | solution.py:146
  276.6 3.2 %copy-start.3 = (bf16[64,2048]{1,0:T(8,128)(2,1)S(1)}, bf16[64,2048]{1,0:T(8,128)(2,1)}, u32[]{:S(2)}) copy-start(bf16[64,2048]{1,0:T(8,128)(2,1)} %reduce-scatter.3.cloned.1.call-done) | copy-start | bytes 786436
Sparse Core Ops, SparseCore 0:
  31.1 37.6 reduce-scatter.2
  210.8 52.2 reduce-scatter.4
